TPU v7x, 32 devices: a whole 2x2x4 slice. The times are simulated.
32 devices in a mesh: fs: 8 (over z, x), tp: 4 (over y, core).
Axes of the slice: x: 2, y: 2, z: 4, core: 2. Of those that a mesh axis runs over, the one named last changes fastest.
Arguments:
- q_latent: bfloat16 [6144, 512], P('fs'), may hold values from -6 to 6
- q_grad: bfloat16 [6144, 3072], P('fs', 'tp'), may hold values from -6 to 6
- uq_master: float32 [512, 3072], P('fs', 'tp'), may hold values from -6 to 6
- uq_basis: bfloat16 [512, 256], P('fs'), may hold values from -4 to 4
- uq_first: float32 [256, 3072], P('fs', 'tp'), may hold values from -3 to 3
- uq_second: float32 [256, 3072], P('fs', 'tp'), may hold values from 0.1 to 1
- kv_latent: bfloat16 [6144, 512], P('fs'), may hold values from -6 to 6
- k_grad: bfloat16 [6144, 2048], P('fs', 'tp'), may hold values from -6 to 6
- uk_master: float32 [512, 2048], P('fs', 'tp'), may hold values from -6 to 6
- uk_basis: bfloat16 [512, 256], P('fs'), may hold values from -4 to 4
- uk_first: float32 [256, 2048], P('fs', 'tp'), may hold values from -3 to 3
- uk_second: float32 [256, 2048], P('fs', 'tp'), may hold values from 0.1 to 1
Outputs:
- uq_first_new: float32 [256, 3072], P('fs', 'tp')
- uq_second_new: float32 [256, 3072], P('fs', 'tp')
- uq_step: float32 [512, 3072], P('fs', 'tp')
- uq_copy: bfloat16 [512, 3072], P(None, 'tp')
- uk_first_new: float32 [256, 2048], P('fs', 'tp')
- uk_second_new: float32 [256, 2048], P('fs', 'tp')
- uk_step: float32 [512, 2048], P('fs', 'tp')
- uk_copy: bfloat16 [512, 2048], P(None, 'tp')
All inputs are finite; a program needn't handle non-finite values.
Results may differ from a plain program's by a relative error of at most 0.0071.
Values may be sent and summed in bfloat16 or wider, within the bound.
A program may use at most 64 MiB of HBM per device.

v0:
```python
import jax
import jax.numpy as jnp
from jax import lax
from jax.sharding import PartitionSpec as P

first_decay = 0.8
second_decay = 0.9
step_size = 0.5
mean_guard = 1e-06
root_guard = 1e-08


def across_tokens(left, right):
    return lax.dot_general(
        left, right, (((0,), (0,)), ((), ())), preferred_element_type=jnp.float32
    )


def across_latent(left, right):
    return lax.dot_general(
        left,
        right,
        (((0,), (0,)), ((), ())),
        precision=lax.Precision.HIGHEST,
        preferred_element_type=jnp.float32,
    )


def moment_update(scaled, first_old, second_old):
    first_new = first_decay * first_old + (1.0 - first_decay) * scaled
    second_new = second_decay * second_old + (1.0 - second_decay) * scaled * scaled
    heading = (first_new / (jnp.sqrt(second_new) + root_guard)).astype(jnp.bfloat16)
    return (first_new, second_new, heading)


def body(
    q_latent,
    q_grad,
    uq_master,
    uq_basis,
    uq_first,
    uq_second,
    kv_latent,
    k_grad,
    uk_master,
    uk_basis,
    uk_first,
    uk_second,
):
    q_width = q_grad.shape[1]
    q_whole, k_whole = (
        lax.all_gather(uq_basis, "fs", axis=0, tiled=True),
        lax.all_gather(uk_basis, "fs", axis=0, tiled=True),
    )
    q_factor = q_whole.astype(jnp.float32)
    k_factor = k_whole.astype(jnp.float32)
    q_partial = across_tokens(q_latent, q_grad)
    k_partial = across_tokens(kv_latent, k_grad)
    projected = lax.psum_scatter(
        jnp.concatenate(
            [across_latent(q_factor, q_partial), across_latent(k_factor, k_partial)], axis=1
        ),
        "fs",
        scatter_dimension=0,
        tiled=True,
    )
    squares_sum = lax.psum(jnp.sum(projected * projected), ("fs", "tp"))
    entry_count = (
        projected.shape[0] * projected.shape[1] * lax.axis_size("fs") * lax.axis_size("tp")
    )
    root_mean = jnp.sqrt(squares_sum / entry_count + mean_guard)
    scaled = projected / root_mean
    uq_first_new, uq_second_new, q_heading = moment_update(scaled[:, :q_width], uq_first, uq_second)
    uk_first_new, uk_second_new, k_heading = moment_update(scaled[:, q_width:], uk_first, uk_second)
    q_dir, k_dir = (
        lax.all_gather(q_heading, "fs", axis=0, tiled=True),
        lax.all_gather(k_heading, "fs", axis=0, tiled=True),
    )
    uq_step = jnp.dot(uq_basis, q_dir, preferred_element_type=jnp.float32)
    uk_step = jnp.dot(uk_basis, k_dir, preferred_element_type=jnp.float32)
    q_fresh = (uq_master - step_size * uq_step).astype(jnp.bfloat16)
    k_fresh = (uk_master - step_size * uk_step).astype(jnp.bfloat16)
    uq_copy, uk_copy = (
        lax.all_gather(q_fresh, "fs", axis=0, tiled=True),
        lax.all_gather(k_fresh, "fs", axis=0, tiled=True),
    )
    return (
        uq_first_new,
        uq_second_new,
        uq_step,
        uq_copy,
        uk_first_new,
        uk_second_new,
        uk_step,
        uk_copy,
    )


def solution(mesh):
    return jax.shard_map(
        body,
        mesh=mesh,
        in_specs=(
            P("fs", None),
            P("fs", "tp"),
            P("fs", "tp"),
            P("fs", None),
            P("fs", "tp"),
            P("fs", "tp"),
            P("fs", None),
            P("fs", "tp"),
            P("fs", "tp"),
            P("fs", None),
            P("fs", "tp"),
            P("fs", "tp"),
        ),
        out_specs=(
            P("fs", "tp"),
            P("fs", "tp"),
            P("fs", "tp"),
            P(None, "tp"),
            P("fs", "tp"),
            P("fs", "tp"),
            P("fs", "tp"),
            P(None, "tp"),
        ),
        check_vma=False,
    )
```

profile of v0, /device:TPU:0, one launch (start us, length us, event | category | flops | bytes accessed | tf_op | source)
XLA Modules:
  0.0 323.5 jit_solution(11529704585300049106)
XLA Ops:
  7.2 0.0 reduce-scatter.4.cloned.1.call-start
  7.2 32.9 %all_gather.18 = bf16[512,256]{1,0:T(8,128)(2,1)S(1)} all-gather(bf16[64,256]{1,0:T(8,128)(2,1)} %param.15), channel_id=1, replica_groups=mesh['fs'=8,'tp'=4] {'fs'}, dimensions={0}, use_global_device_ids=true | all-gather | bytes 294912 | tf_op jit(solution)/shard_map/all_gather | solution.py:52
  40.2 30.9 %all_gather.19 = bf16[512,256]{1,0:T(8,128)(2,1)S(1)} all-gather(bf16[64,256]{1,0:T(8,128)(2,1)} %param.21), channel_id=1, replica_groups=mesh['fs'=8,'tp'=4] {'fs'}, dimensions={0}, use_global_device_ids=true | all-gather | bytes 294912 | tf_op jit(solution)/shard_map/all_gather | solution.py:53
  71.1 1.9 fusion.4
  73.1 1.4 convolution_bitcast_fusion
  74.5 0.6 fusion.5
  75.1 1.0 convolution_bitcast_fusion.1
  76.1 0.1 pad_maximum_fusion
  76.2 1.5 copy.39
  77.7 0.0 reduce-scatter.4.cloned.1.call-update
  77.8 66.1 %reduce-scatter.4.cloned.1.call-done = f32[32,1280]{1,0:T(8,128)} async-done(((f32[256,1280]{1,0:T(8,128)}), f32[32,1280]{1,0:T(8,128)}) %reduce-scatter.4.cloned.1.call-update) | async-done | bytes 163856 | tf_op jit(solution)/shard_map/reduce_scatter | solution.py:59
  143.9 1.2 copy.40
  145.1 0.8 multiply_reduce_fusion
  145.9 39.9 %psum.7 = f32[]{:T(128)} all-reduce(f32[]{:T(128)} %multiply_reduce_fusion), channel_id=1, replica_groups=mesh['fs'=8,'tp'=4] {'fs','tp'}, use_global_device_ids=true, to_apply=%region_2.0 | all-reduce | flops 1 | bytes 8 | tf_op jit(solution)/shard_map/psum | solution.py:67
  186.5 0.7 divide_convert_fusion
  187.3 31.3 %all_gather.20 = bf16[256,768]{1,0:T(8,128)(2,1)S(1)} all-gather(bf16[32,768]{1,0:T(8,128)(2,1)S(1)} %get-tuple-element.27), channel_id=1, replica_groups=mesh['fs'=8,'tp'=4] {'fs'}, dimensions={0}, use_global_device_ids=true | all-gather | bytes 442368 | tf_op jit(solution)/shard_map/all_gather | solution.py:76
  218.5 0.9 subtract_convert_fusion
  219.4 32.1 %all_gather.21 = bf16[512,768]{1,0:T(8,128)(2,1)S(1)} all-gather(bf16[64,768]{1,0:T(8,128)(2,1)S(1)} %get-tuple-element.30), channel_id=1, replica_groups=mesh['fs'=8,'tp'=4] {'fs'}, dimensions={0}, use_global_device_ids=true | all-gather | bytes 884736 | tf_op jit(solution)/shard_map/all_gather | solution.py:84
  251.5 0.7 divide_convert_fusion.1
  252.2 30.8 %all_gather.22 = bf16[256,512]{1,0:T(8,128)(2,1)S(1)} all-gather(bf16[32,512]{1,0:T(8,128)(2,1)S(1)} %get-tuple-element.24), channel_id=1, replica_groups=mesh['fs'=8,'tp'=4] {'fs'}, dimensions={0}, use_global_device_ids=true | all-gather | bytes 294912 | tf_op jit(solution)/shard_map/all_gather | solution.py:77
  283.0 0.8 subtract_convert_fusion.1
  283.8 31.2 %all_gather.23 = bf16[512,512]{1,0:T(8,128)(2,1)S(1)} all-gather(bf16[64,512]{1,0:T(8,128)(2,1)S(1)} %get-tuple-element.32), channel_id=1, replica_groups=mesh['fs'=8,'tp'=4] {'fs'}, dimensions={0}, use_global_device_ids=true | all-gather | bytes 589824 | tf_op jit(solution)/shard_map/all_gather | solution.py:85
  315.0 0.9 copy.43
  315.9 0.8 copy.44
  (25 shorter events, 0.1 us)
Async XLA Ops:
  7.2 63.9 %copy-start = (bf16[768,768]{1,0:T(8,128)(2,1)S(1)}, bf16[768,768]{1,0:T(8,128)(2,1)}, u32[]{:S(2)}) copy-start(bf16[768,768]{1,0:T(8,128)(2,1)} %param.13) | copy-start | bytes 3538948
  7.2 136.7 %reduce-scatter.4.cloned.1.call-start = ((), (), s32[]{:S(2)}) async-start(), calls=%async_computation.1 | async-start | bytes 1474560 | tf_op jit(solution)/shard_map/reduce_scatter | solution.py:59
  73.1 1.4 copy-start.1
  73.1 1.4 copy-start.2
  77.7 108.8 %copy-start.8 = (f32[32,768]{1,0:T(8,128)S(1)}, f32[32,768]{1,0:T(8,128)}, u32[]{:S(2)}) copy-start(f32[32,768]{1,0:T(8,128)} %param.17) | copy-start | bytes 294916
  77.7 108.8 %copy-start.9 = (f32[32,768]{1,0:T(8,128)S(1)}, f32[32,768]{1,0:T(8,128)}, u32[]{:S(2)}) copy-start(f32[32,768]{1,0:T(8,128)} %param.16) | copy-start | bytes 294916
  77.8 140.8 %copy-start.4 = (f32[64,768]{1,0:T(8,128)S(1)}, f32[64,768]{1,0:T(8,128)}, u32[]{:S(2)}) copy-start(f32[64,768]{1,0:T(8,128)} %param.14) | copy-start | bytes 589828
  77.8 140.7 %copy-start.6 = (bf16[64,256]{1,0:T(8,128)(2,1)S(1)}, bf16[64,256]{1,0:T(8,128)(2,1)}, u32[]{:S(2)}) copy-start(bf16[64,256]{1,0:T(8,128)(2,1)} %param.15) | copy-start | bytes 98308
  143.9 42.6 %copy-start.3 = (f32[32,1280]{1,0:T(8,128)S(1)}, f32[32,1280]{1,0:T(8,128)}, u32[]{:S(2)}) copy-start(f32[32,1280]{1,0:T(8,128)} %reduce-scatter.4.cloned.1.call-done) | copy-start | bytes 491524
  186.5 65.0 %copy-start.10 = (f32[32,512]{1,0:T(8,128)S(1)}, f32[32,512]{1,0:T(8,128)}, u32[]{:S(2)}) copy-start(f32[32,512]{1,0:T(8,128)} %param.23) | copy-start | bytes 196612
  186.5 65.0 %copy-start.11 = (f32[32,512]{1,0:T(8,128)S(1)}, f32[32,512]{1,0:T(8,128)}, u32[]{:S(2)}) copy-start(f32[32,512]{1,0:T(8,128)} %param.22) | copy-start | bytes 196612
  218.5 64.5 %copy-start.5 = (f32[64,512]{1,0:T(8,128)S(1)}, f32[64,512]{1,0:T(8,128)}, u32[]{:S(2)}) copy-start(f32[64,512]{1,0:T(8,128)} %param.20) | copy-start | bytes 393220
  218.5 64.5 %copy-start.7 = (bf16[64,256]{1,0:T(8,128)(2,1)S(1)}, bf16[64,256]{1,0:T(8,128)(2,1)}, u32[]{:S(2)}) copy-start(bf16[64,256]{1,0:T(8,128)(2,1)} %param.21) | copy-start | bytes 98308
Sparse Core Ops, SparseCore 0:
  77.9 65.9 reduce-scatter.3
where the time goes:
time: 324 us; the launch traced here: 323 us
  blocking collectives  229 us (71%)
  waiting for transfers between devices  66.1 us (20%)
  between operations  14.9 us (5%)
  matrix products  6.67 us (2%)
  local copies, waits for them, and re-layouts  4.45 us (1%)
    reduce_scatter x1, waiting for transfers between devices, body(): lax.psum_scatter(jnp.concatenate([across_latent(q_factor, q_partial), acr...  66.1 us
    psum x1, blocking collectives, body(): squares_sum = lax.psum(jnp.sum(projected * projected), ('fs', 'tp'))  39.9 us
    all_gather x1, blocking collectives, body(): lax.all_gather(uq_basis, 'fs', axis=0, tiled=True)  32.9 us
    all_gather x1, blocking collectives, body(): lax.all_gather(q_fresh, 'fs', axis=0, tiled=True)  32.1 us
    all_gather x1, blocking collectives, body(): lax.all_gather(q_heading, 'fs', axis=0, tiled=True)  31.3 us
    all_gather x1, blocking collectives, body(): lax.all_gather(k_fresh, 'fs', axis=0, tiled=True)  31.2 us
    all_gather x1, blocking collectives, body(): lax.all_gather(uk_basis, 'fs', axis=0, tiled=True)  30.9 us
    all_gather x1, blocking collectives, body(): lax.all_gather(k_heading, 'fs', axis=0, tiled=True)  30.8 us
  transfers between devices with their start and end apart: 1, of which 1 were waited for; matrix products, arithmetic and copies ran while one was open for 0% of the time, Pallas kernels for 0%

commit v1 on v0

--- a/solution.py
+++ b/solution.py
@@ -80,8 +80,11 @@
     uk_step = jnp.dot(uk_basis, k_dir, preferred_element_type=jnp.float32)
     q_fresh = (uq_master - step_size * uq_step).astype(jnp.bfloat16)
     k_fresh = (uk_master - step_size * uk_step).astype(jnp.bfloat16)
+    convert_the_stops_all = lambda xx: jnp.concatenate(
+        lax.all_to_all(jnp.stack([xx for _ in range(lax.axis_size("fs"))]), "fs", 0, 0), axis=0
+    )
     uq_copy, uk_copy = (
-        lax.all_gather(q_fresh, "fs", axis=0, tiled=True),
+        convert_the_stops_all(q_fresh),
         lax.all_gather(k_fresh, "fs", axis=0, tiled=True),
     )
     return (

time: 324 us -> 303 us (0.935)
  blocking collectives: 229 us -> 203 us
  starting transfers between devices: 0.04 us -> 4.87 us
    all_gather x1 -> x0, blocking collectives: 32.1 us -> none  [body(): lax.all_gather(q_fresh, 'fs', axis=0, tiled=True)]
    all_gather x1, blocking collectives: 30.8 us -> 36.7 us  [body(): lax.all_gather(k_heading, 'fs', axis=0, tiled=True)]
    all_to_all x0 -> x1, starting transfers between devices: none -> 4.84 us  [body(): lax.all_to_all(jnp.stack([xx for _ in range(lax.axis_size('fs'))]), 'fs',...]
  transfers between devices with their start and end apart: 1 -> 2, of which waited for: 1 -> 1; matrix products, arithmetic and copies ran while one was open for 0% -> 0% of each run, Pallas kernels for 0% -> 0%
where the time goes in v1:
time: 303 us
  blocking collectives  203 us (67%)
  waiting for transfers between devices  66.1 us (22%)
  between operations  14.9 us (5%)
  matrix products  6.67 us (2%)
  local copies, waits for them, and re-layouts  5.37 us (2%)
  starting transfers between devices  4.87 us (2%)
    reduce_scatter x1, waiting for transfers between devices, body(): lax.psum_scatter(jnp.concatenate([across_latent(q_factor, q_partial), acr...  66.1 us
    psum x1, blocking collectives, body(): squares_sum = lax.psum(jnp.sum(projected * projected), ('fs', 'tp'))  39.9 us
    all_gather x1, blocking collectives, body(): lax.all_gather(k_heading, 'fs', axis=0, tiled=True)  36.7 us
    all_gather x1, blocking collectives, body(): lax.all_gather(uq_basis, 'fs', axis=0, tiled=True)  32.9 us
    all_gather x1, blocking collectives, body(): lax.all_gather(k_fresh, 'fs', axis=0, tiled=True)  31.2 us
    all_gather x1, blocking collectives, body(): lax.all_gather(q_heading, 'fs', axis=0, tiled=True)  31.1 us
    all_gather x1, blocking collectives, body(): lax.all_gather(uk_basis, 'fs', axis=0, tiled=True)  30.9 us
  transfers between devices with their start and end apart: 2, of which 1 were waited for; matrix products, arithmetic and copies ran while one was open for 0% of the time, Pallas kernels for 0%

profile of v1, /device:TPU:0, one launch (start us, length us, event | category | flops | bytes accessed | tf_op | source)
XLA Modules:
  0.0 302.9 jit_solution(11147435918126866694)
XLA Ops:
  7.2 0.0 reduce-scatter.4.cloned.1.call-start
  7.2 32.9 %all_gather.15 = bf16[512,256]{1,0:T(8,128)(2,1)S(1)} all-gather(bf16[64,256]{1,0:T(8,128)(2,1)} %param.15), channel_id=1, replica_groups=mesh['fs'=8,'tp'=4] {'fs'}, dimensions={0}, use_global_device_ids=true | all-gather | bytes 294912 | tf_op jit(solution)/shard_map/all_gather | solution.py:52
  40.2 30.9 %all_gather.16 = bf16[512,256]{1,0:T(8,128)(2,1)S(1)} all-gather(bf16[64,256]{1,0:T(8,128)(2,1)} %param.21), channel_id=1, replica_groups=mesh['fs'=8,'tp'=4] {'fs'}, dimensions={0}, use_global_device_ids=true | all-gather | bytes 294912 | tf_op jit(solution)/shard_map/all_gather | solution.py:53
  71.1 1.9 fusion.4
  73.1 1.4 convolution_bitcast_fusion
  74.5 0.6 fusion.5
  75.1 1.0 convolution_bitcast_fusion.1
  76.1 0.1 pad_maximum_fusion
  76.2 1.5 copy.39
  77.8 66.1 %reduce-scatter.4.cloned.1.call-done = f32[32,1280]{1,0:T(8,128)} async-done(((f32[256,1280]{1,0:T(8,128)}), f32[32,1280]{1,0:T(8,128)}) %reduce-scatter.4.cloned.1.call-update) | async-done | bytes 163856 | tf_op jit(solution)/shard_map/reduce_scatter | solution.py:59
  143.9 1.2 copy.40
  145.1 0.8 multiply_reduce_fusion
  145.9 39.9 %psum.7 = f32[]{:T(128)} all-reduce(f32[]{:T(128)} %multiply_reduce_fusion), channel_id=1, replica_groups=mesh['fs'=8,'tp'=4] {'fs','tp'}, use_global_device_ids=true, to_apply=%region_2.0 | all-reduce | flops 1 | bytes 8 | tf_op jit(solution)/shard_map/psum | solution.py:67
  186.5 0.7 divide_convert_fusion
  187.2 31.1 %all_gather.17 = bf16[256,768]{1,0:T(8,128)(2,1)S(1)} all-gather(bf16[32,768]{1,0:T(8,128)(2,1)S(1)} %get-tuple-element.27), channel_id=1, replica_groups=mesh['fs'=8,'tp'=4] {'fs'}, dimensions={0}, use_global_device_ids=true | all-gather | bytes 442368 | tf_op jit(solution)/shard_map/all_gather | solution.py:76
  218.3 0.9 subtract_convert_fusion
  219.2 0.9 stack.2
  220.1 4.8 %all-to-all-start = ((bf16[8,64,768]{2,1,0:T(8,128)(2,1)}), bf16[8,64,768]{2,1,0:T(8,128)(2,1)S(1)}, u32[]{:S(2)}, u32[]{:S(2)}) async-start(bf16[8,64,768]{2,1,0:T(8,128)(2,1)} %stack.2), calls=%async_computation | async-start | bytes 1572864 | tf_op jit(solution)/shard_map/all_to_all | solution.py:84
  225.0 0.7 divide_convert_fusion.1
  225.7 36.7 %all_gather.18 = bf16[256,512]{1,0:T(8,128)(2,1)S(1)} all-gather(bf16[32,512]{1,0:T(8,128)(2,1)S(1)} %get-tuple-element.24), channel_id=1, replica_groups=mesh['fs'=8,'tp'=4] {'fs'}, dimensions={0}, use_global_device_ids=true | all-gather | bytes 294912 | tf_op jit(solution)/shard_map/all_gather | solution.py:77
  262.4 0.8 subtract_convert_fusion.1
  263.2 31.2 %all_gather.19 = bf16[512,512]{1,0:T(8,128)(2,1)S(1)} all-gather(bf16[64,512]{1,0:T(8,128)(2,1)S(1)} %get-tuple-element.32), channel_id=1, replica_groups=mesh['fs'=8,'tp'=4] {'fs'}, dimensions={0}, use_global_device_ids=true | all-gather | bytes 589824 | tf_op jit(solution)/shard_map/all_gather | solution.py:88
  294.3 0.9 copy.43
  295.2 0.8 copy.44
  (27 shorter events, 0.1 us)
Async XLA Ops:
  7.2 63.9 %copy-start = (bf16[768,768]{1,0:T(8,128)(2,1)S(1)}, bf16[768,768]{1,0:T(8,128)(2,1)}, u32[]{:S(2)}) copy-start(bf16[768,768]{1,0:T(8,128)(2,1)} %param.13) | copy-start | bytes 3538948
  7.2 136.7 %reduce-scatter.4.cloned.1.call-start = ((), (), s32[]{:S(2)}) async-start(), calls=%async_computation.2 | async-start | bytes 1474560 | tf_op jit(solution)/shard_map/reduce_scatter | solution.py:59
  73.1 1.4 copy-start.1
  73.1 1.4 copy-start.2
  77.7 108.7 %copy-start.8 = (f32[32,768]{1,0:T(8,128)S(1)}, f32[32,768]{1,0:T(8,128)}, u32[]{:S(2)}) copy-start(f32[32,768]{1,0:T(8,128)} %param.17) | copy-start | bytes 294916
  77.7 108.8 %copy-start.9 = (f32[32,768]{1,0:T(8,128)S(1)}, f32[32,768]{1,0:T(8,128)}, u32[]{:S(2)}) copy-start(f32[32,768]{1,0:T(8,128)} %param.16) | copy-start | bytes 294916
  77.8 140.5 %copy-start.4 = (f32[64,768]{1,0:T(8,128)S(1)}, f32[64,768]{1,0:T(8,128)}, u32[]{:S(2)}) copy-start(f32[64,768]{1,0:T(8,128)} %param.14) | copy-start | bytes 589828
  77.8 140.5 %copy-start.6 = (bf16[64,256]{1,0:T(8,128)(2,1)S(1)}, bf16[64,256]{1,0:T(8,128)(2,1)}, u32[]{:S(2)}) copy-start(bf16[64,256]{1,0:T(8,128)(2,1)} %param.15) | copy-start | bytes 98308
  143.9 42.6 %copy-start.3 = (f32[32,1280]{1,0:T(8,128)S(1)}, f32[32,1280]{1,0:T(8,128)}, u32[]{:S(2)}) copy-start(f32[32,1280]{1,0:T(8,128)} %reduce-scatter.4.cloned.1.call-done) | copy-start | bytes 491524
  219.2 5.8 %copy-start.10 = (f32[32,512]{1,0:T(8,128)S(1)}, f32[32,512]{1,0:T(8,128)}, u32[]{:S(2)}) copy-start(f32[32,512]{1,0:T(8,128)} %param.23) | copy-start | bytes 196612
  219.2 5.8 %copy-start.11 = (f32[32,512]{1,0:T(8,128)S(1)}, f32[32,512]{1,0:T(8,128)}, u32[]{:S(2)}) copy-start(f32[32,512]{1,0:T(8,128)} %param.22) | copy-start | bytes 196612
  220.1 42.2 %copy-start.5 = (f32[64,512]{1,0:T(8,128)S(1)}, f32[64,512]{1,0:T(8,128)}, u32[]{:S(2)}) copy-start(f32[64,512]{1,0:T(8,128)} %param.20) | copy-start | bytes 393220
  220.1 42.2 %copy-start.7 = (bf16[64,256]{1,0:T(8,128)(2,1)S(1)}, bf16[64,256]{1,0:T(8,128)(2,1)}, u32[]{:S(2)}) copy-start(bf16[64,256]{1,0:T(8,128)(2,1)} %param.21) | copy-start | bytes 98308
  220.1 74.2 %all-to-all-start = ((bf16[8,64,768]{2,1,0:T(8,128)(2,1)}), bf16[8,64,768]{2,1,0:T(8,128)(2,1)S(1)}, u32[]{:S(2)}, u32[]{:S(2)}) async-start(bf16[8,64,768]{2,1,0:T(8,128)(2,1)} %stack.2), calls=%async_computation | async-start | bytes 1572864 | tf_op jit(solution)/shard_map/all_to_all | solution.py:84
Sparse Core Ops, SparseCore 0:
  77.9 65.9 reduce-scatter.3
